TPU v7x, 32 devices: a whole 2x2x4 slice. The times are simulated.
32 devices in a mesh: sp: 16 (over z, y, x), tp: 2 (over core).
Axes of the slice: x: 2, y: 2, z: 4, core: 2. Of those that a mesh axis runs over, the one named last changes fastest.
Arguments:
- tokens: bfloat16 [2048, 1024], P('sp', 'tp'), may hold values from -6 to 6
- norm_gain: float32 [1024], P('tp'), may hold values from 0.1 to 1.9
- query_weight: bfloat16 [1024, 1024], P('sp', 'tp'), may hold values from -0.1875 to 0.1875
- key_weight: bfloat16 [1024, 512], P('sp', 'tp'), may hold values from -0.1875 to 0.1875
- value_weight: bfloat16 [1024, 512], P('sp', 'tp'), may hold values from -0.1875 to 0.1875
- conv_in_weight: bfloat16 [1024, 1024], P('sp', 'tp'), may hold values from -0.1875 to 0.1875
- pre_weight: bfloat16 [1024, 1024], P('sp', 'tp'), may hold values from -0.1875 to 0.1875
- post_weight: bfloat16 [1024, 1024], P('sp', 'tp'), may hold values from -0.1875 to 0.1875
- attn_gate_weight: bfloat16 [1024, 1024], P('sp', 'tp'), may hold values from -0.1875 to 0.1875
- conv_gate_weight: bfloat16 [1024, 1024], P('sp', 'tp'), may hold values from -0.1875 to 0.1875
- sink_logit: float32 [16], P('tp'), may hold values from 1 to 5
- conv_taps: float32 [3, 1024], P(None, 'tp'), may hold values from -3 to 3
- attn_out_weight: bfloat16 [1024, 1024], P('tp', 'sp'), may hold values from -1 to 1
- conv_out_weight: bfloat16 [1024, 1024], P('tp', 'sp'), may hold values from -0.1875 to 0.1875
Outputs:
- merged: bfloat16 [2048, 1024], P('sp', 'tp')
All inputs are finite; a program needn't handle non-finite values.
Results may differ from a plain program's by a relative error of at most 0.003.
Values may be sent and summed in bfloat16 or wider, within the bound.
A program may use at most 64 MiB of HBM per device.

v0:
```python
import jax
import jax.numpy as jnp
from jax import lax
from jax.sharding import PartitionSpec as P

HEAD_DIM = 64
WINDOW = 64


epsilon = 1e-06
negative = -1e30


def folded(shard, axis, dim, absorb, state):
    everything = jax.tree.map(lambda a: lax.all_gather(a, axis, axis=dim, tiled=True), shard)
    return absorb(state, everything, jnp.int32(0))


def for_sending(shard):
    def short(part):
        return part.astype(jnp.bfloat16) if part.dtype == jnp.float32 else part

    return jax.tree.map(short, shard)


def extended(shard, sides, width, wrap):
    for axis, dim in sides:
        devices, length = lax.axis_size(axis), shard.shape[dim]
        up = [(i, (i + 1) % devices) for i in range(devices if wrap else devices - 1)]
        down = [(j, i) for i, j in up]
        last = lax.slice_in_dim(shard, length - width, length, axis=dim)
        first = lax.slice_in_dim(shard, 0, width, axis=dim)
        before = lax.ppermute(last, axis, up)
        after = lax.ppermute(first, axis, down)
        shard = jnp.concatenate([before, shard, after], axis=dim)
    return shard


def summed_rows(product, width, axis):
    whole = product(jnp.int32(0), width * lax.axis_size(axis))
    return lax.psum_scatter(whole, axis, scatter_dimension=0, tiled=True)


def window_mix(queries, key_rows, value_rows, sink_cols, first, seq_total):
    score_scale = queries.shape[-1] ** (-0.5)
    scores = (
        jnp.einsum("qhgd,khd->hgqk", queries, key_rows, preferred_element_type=jnp.float32)
        * score_scale
    )
    qpos = first + jnp.arange(queries.shape[0], dtype=jnp.int32)
    kpos = first - WINDOW + jnp.arange(key_rows.shape[0], dtype=jnp.int32)
    allowed = (
        (jnp.abs(qpos[:, None] - kpos[None, :]) <= WINDOW)
        & (kpos >= 0)[None, :]
        & (kpos < seq_total)[None, :]
    )
    scores = jnp.where(allowed, scores, negative)
    column = jnp.broadcast_to(sink_cols[:, :, None, None], scores.shape[:-1] + (1,))
    weights_soft = jax.nn.softmax(jnp.concatenate([scores, column], axis=-1), axis=-1)[..., :-1]
    return jnp.einsum(
        "hgqk,khd->qhgd",
        weights_soft,
        value_rows.astype(jnp.float32),
        precision=lax.Precision.HIGHEST,
    )


def short_conv(padded, conv_taps):
    return (
        conv_taps[0][None, :] * padded[:-2]
        + conv_taps[1][None, :] * padded[1:-1]
        + conv_taps[2][None, :] * padded[2:]
    )


def per_device(
    tokens,
    norm_gain,
    query_weight,
    key_weight,
    value_weight,
    conv_in_weight,
    pre_weight,
    post_weight,
    attn_gate_weight,
    conv_gate_weight,
    sink_logit,
    conv_taps,
    attn_out_weight,
    conv_out_weight,
):
    tok_rows = tokens.shape[0]
    widened = tokens.astype(jnp.float32)
    row_sums = lax.psum(jnp.sum(widened * widened, axis=1), "tp")
    features = tokens.shape[1] * lax.axis_size("tp")
    normed = (
        widened * lax.rsqrt(row_sums[:, None] / features + epsilon) * norm_gain[None, :]
    ).astype(jnp.bfloat16)
    collected = (
        lax.all_gather(query_weight, "sp", axis=0, tiled=True),
        lax.all_gather(key_weight, "sp", axis=0, tiled=True),
        lax.all_gather(value_weight, "sp", axis=0, tiled=True),
        lax.all_gather(conv_in_weight, "sp", axis=0, tiled=True),
        lax.all_gather(pre_weight, "sp", axis=0, tiled=True),
        lax.all_gather(post_weight, "sp", axis=0, tiled=True),
        lax.all_gather(attn_gate_weight, "sp", axis=0, tiled=True),
        lax.all_gather(conv_gate_weight, "sp", axis=0, tiled=True),
    )
    stacked = jnp.concatenate(collected, axis=1)

    def add_rows(carry_sum, segment, first):
        rows_here = lax.dynamic_slice_in_dim(stacked, first, segment.shape[1], 0)
        return carry_sum + jnp.dot(segment, rows_here, preferred_element_type=jnp.float32)

    projected = folded(
        normed, "tp", 1, add_rows, jnp.zeros((tok_rows, stacked.shape[1]), jnp.float32)
    )
    pieces = []
    offset = 0
    for weight in collected:
        pieces.append(projected[:, offset : offset + weight.shape[1]])
        offset = offset + weight.shape[1]
    queries, key_rows, value_rows, conv_in, pre_gate, post_gate = [
        part_rows.astype(jnp.bfloat16) for part_rows in pieces[:6]
    ]
    attn_gate = pieces[6]
    conv_gate = pieces[7]
    conv_mix = (pre_gate.astype(jnp.float32) * conv_in.astype(jnp.float32)).astype(jnp.bfloat16)
    kv_width = key_rows.shape[1]
    kv_pad = extended(
        for_sending(jnp.concatenate([key_rows, value_rows], axis=1)), (("sp", 0),), WINDOW, False
    )
    key_pad = kv_pad[:, :kv_width]
    value_pad = kv_pad[:, kv_width:]
    conv_pad = extended(conv_mix, (("sp", 0),), 1, False)
    kv_local = kv_width // HEAD_DIM
    group_size = queries.shape[1] // kv_width
    first_row = lax.axis_index("sp") * tok_rows
    attended = window_mix(
        queries.reshape(tok_rows, kv_local, group_size, HEAD_DIM),
        key_pad.reshape(-1, kv_local, HEAD_DIM),
        value_pad.reshape(-1, kv_local, HEAD_DIM),
        sink_logit.reshape(kv_local, group_size),
        first_row,
        tok_rows * lax.axis_size("sp"),
    )
    attended = attended.reshape(tok_rows, -1).astype(jnp.bfloat16)
    conv_out = (
        post_gate.astype(jnp.float32) * short_conv(conv_pad.astype(jnp.float32), conv_taps)
    ).astype(jnp.bfloat16)
    attn_full, conv_full = (
        lax.all_gather(attn_out_weight, "sp", axis=1, tiled=True),
        lax.all_gather(conv_out_weight, "sp", axis=1, tiled=True),
    )

    def attn_term(first, number):
        columns = lax.dynamic_slice_in_dim(attn_full, first, number, 1)
        return jnp.dot(attended, columns, preferred_element_type=jnp.float32).T

    def conv_term(first, number):
        columns = lax.dynamic_slice_in_dim(conv_full, first, number, 1)
        return jnp.dot(conv_out, columns, preferred_element_type=jnp.float32).T

    out_rows = attn_gate.shape[1]

    def both_terms(first, number):
        return jnp.concatenate([attn_term(first, number), conv_term(first, number)], axis=1)

    summed = summed_rows(both_terms, out_rows, "tp")
    branch_attn = summed[:, :tok_rows].T
    branch_conv = summed[:, tok_rows:].T
    return (
        jax.nn.sigmoid(attn_gate) * branch_attn + jax.nn.sigmoid(conv_gate) * branch_conv
    ).astype(jnp.bfloat16)


def solution(mesh):
    return jax.shard_map(
        per_device,
        mesh=mesh,
        in_specs=(
            P("sp", "tp"),
            P("tp"),
            P("sp", "tp"),
            P("sp", "tp"),
            P("sp", "tp"),
            P("sp", "tp"),
            P("sp", "tp"),
            P("sp", "tp"),
            P("sp", "tp"),
            P("sp", "tp"),
            P("tp"),
            P(None, "tp"),
            P("tp", "sp"),
            P("tp", "sp"),
        ),
        out_specs=P("sp", "tp"),
        check_vma=False,
    )
```

profile of v0, /device:TPU:0, one launch (start us, length us, event | category | flops | bytes accessed | tf_op | source)
XLA Modules:
  0.0 486.1 jit_solution(2736074384034451135)
XLA Ops:
  12.1 45.7 %all_gather.35 = bf16[1024,256]{1,0:T(8,128)(2,1)S(1)} all-gather(bf16[64,256]{1,0:T(8,128)(2,1)} %param.17), channel_id=1, replica_groups=mesh['sp'=16,'tp'=2] {'sp'}, dimensions={0}, use_global_device_ids=true | all-gather | bytes 557056 | tf_op jit(solution)/shard_map/all_gather | solution.py:101
  57.7 40.2 %all_gather.36 = bf16[1024,256]{1,0:T(8,128)(2,1)S(1)} all-gather(bf16[64,256]{1,0:T(8,128)(2,1)} %param.18), channel_id=1, replica_groups=mesh['sp'=16,'tp'=2] {'sp'}, dimensions={0}, use_global_device_ids=true | all-gather | bytes 557056 | tf_op jit(solution)/shard_map/all_gather | solution.py:102
  97.9 1.0 fusion.4
  99.0 2.5 psum.7
  101.4 1.0 fusion.6
  102.5 2.0 all_gather.33
  104.5 1.3 broadcast_in_dim.27
  105.8 1.4 fusion.35
  108.0 2.3 constant_dynamic-update-slice_fusion.7
  112.1 15.5 %all-gather.11.cloned.1.call-done = bf16[1024,512]{1,0:T(8,128)(2,1)} async-done(((bf16[64,512]{1,0:T(8,128)(2,1)}), bf16[1024,512]{1,0:T(8,128)(2,1)}) %all-gather.11.cloned.1.call-update) | async-done | bytes 1048592 | tf_op jit(solution)/shard_map/all_gather | solution.py:103
  127.6 2.3 constant_dynamic-update-slice_fusion.4
  129.9 54.4 %all-gather.13.cloned.1.call-done = bf16[1024,512]{1,0:T(8,128)(2,1)} async-done(((bf16[64,512]{1,0:T(8,128)(2,1)}), bf16[1024,512]{1,0:T(8,128)(2,1)}) %all-gather.13.cloned.1.call-update) | async-done | bytes 1048592 | tf_op jit(solution)/shard_map/all_gather | solution.py:104
  184.4 2.3 constant_dynamic-update-slice_fusion.3
  186.6 54.3 %all-gather.15.cloned.1.call-done = bf16[1024,512]{1,0:T(8,128)(2,1)} async-done(((bf16[64,512]{1,0:T(8,128)(2,1)}), bf16[1024,512]{1,0:T(8,128)(2,1)}) %all-gather.15.cloned.1.call-update) | async-done | bytes 1048592 | tf_op jit(solution)/shard_map/all_gather | solution.py:105
  240.9 2.3 constant_dynamic-update-slice_fusion.2
  243.2 54.3 %all-gather.17.cloned.1.call-done = bf16[1024,512]{1,0:T(8,128)(2,1)} async-done(((bf16[64,512]{1,0:T(8,128)(2,1)}), bf16[1024,512]{1,0:T(8,128)(2,1)}) %all-gather.17.cloned.1.call-update) | async-done | bytes 1048592 | tf_op jit(solution)/shard_map/all_gather | solution.py:106
  297.5 2.3 constant_dynamic-update-slice_fusion.1
  299.8 54.2 %all-gather.19.cloned.1.call-done = bf16[1024,512]{1,0:T(8,128)(2,1)} async-done(((bf16[64,512]{1,0:T(8,128)(2,1)}), bf16[1024,512]{1,0:T(8,128)(2,1)}) %all-gather.19.cloned.1.call-update) | async-done | bytes 1048592 | tf_op jit(solution)/shard_map/all_gather | solution.py:107
  354.1 2.3 constant_dynamic-update-slice_fusion
  356.4 4.2 fusion.36
  361.4 3.4 collective-permute-start.2
  364.7 1.3 collective-permute-start.3
  366.7 5.2 %collective-permute-start = (bf16[64,512]{1,0:T(8,128)(2,1)}, bf16[64,512]{1,0:T(8,128)(2,1)}, u32[]{:S(2)}, u32[]{:S(2)}) collective-permute-start(bf16[64,512]{1,0:T(8,128)(2,1)} %get-tuple-element.9), channel_id=1, source_target_pairs={{0,2},{2,4},{4,6},{6,8},{8,10},{10,12},{12,14},{14,16},{16,18},{18... | collective-permute-start | bytes 196616 | tf_op jit(solution)/shard_map/ppermute | solution.py:33
  371.8 1.3 collective-permute-start.1
  373.9 36.9 %all-gather.23.cloned.1.call-done = bf16[512,1024]{0,1:T(8,128)(2,1)} async-done(((bf16[512,64]{0,1:T(8,128)(2,1)}), bf16[512,1024]{0,1:T(8,128)(2,1)}) %all-gather.23.cloned.1.call-update) | async-done | bytes 1048592 | tf_op jit(solution)/shard_map/all_gather | solution.py:153
  410.8 1.7 convolution_bitcast_fusion
  413.8 1.3 fusion.37
  417.3 50.3 %all-gather.21.cloned.1.call-done = bf16[512,1024]{0,1:T(8,128)(2,1)} async-done(((bf16[512,64]{0,1:T(8,128)(2,1)}), bf16[512,1024]{0,1:T(8,128)(2,1)}) %all-gather.21.cloned.1.call-update) | async-done | bytes 1048592 | tf_op jit(solution)/shard_map/all_gather | solution.py:152
  467.6 1.7 convolution_bitcast_fusion.1
  469.3 1.1 pad_maximum_fusion
  470.4 7.4 %reduce-scatter.2.cloned.1.call-done = f32[512,256]{0,1:T(8,128)} async-done(((f32[1024,256]{0,1:T(8,128)}), f32[512,256]{0,1:T(8,128)}) %reduce-scatter.2.cloned.1.call-update) | async-done | bytes 524304 | tf_op jit(solution)/shard_map/reduce_scatter | solution.py:41
  477.8 1.8 fusion.9
  (44 shorter events, 13.6 us)
Async XLA Ops:
  6.5 101.4 %all-gather.9.cloned.1.call-start = ((), (), s32[]{:S(2)}) async-start(), calls=%async_computation.1 | async-start | bytes 1114112 | tf_op jit(solution)/shard_map/all_gather | solution.py:100
  7.3 120.4 %all-gather.11.cloned.1.call-start = ((), (), s32[]{:S(2)}) async-start(), calls=%async_computation.2 | async-start | bytes 1114112 | tf_op jit(solution)/shard_map/all_gather | solution.py:103
  8.0 176.4 %all-gather.13.cloned.1.call-start = ((), (), s32[]{:S(2)}) async-start(), calls=%async_computation.3 | async-start | bytes 1114112 | tf_op jit(solution)/shard_map/all_gather | solution.py:104
  8.7 232.2 %all-gather.15.cloned.1.call-start = ((), (), s32[]{:S(2)}) async-start(), calls=%async_computation.4 | async-start | bytes 1114112 | tf_op jit(solution)/shard_map/all_gather | solution.py:105
  9.3 288.2 %all-gather.17.cloned.1.call-start = ((), (), s32[]{:S(2)}) async-start(), calls=%async_computation.5 | async-start | bytes 1114112 | tf_op jit(solution)/shard_map/all_gather | solution.py:106
  9.9 344.2 %all-gather.19.cloned.1.call-start = ((), (), s32[]{:S(2)}) async-start(), calls=%async_computation.6 | async-start | bytes 1114112 | tf_op jit(solution)/shard_map/all_gather | solution.py:107
  10.5 400.4 %all-gather.23.cloned.1.call-start = ((), (), s32[]{:S(2)}) async-start(), calls=%async_computation.8 | async-start | bytes 1114112 | tf_op jit(solution)/shard_map/all_gather | solution.py:153
  11.2 456.3 %all-gather.21.cloned.1.call-start = ((), (), s32[]{:S(2)}) async-start(), calls=%async_computation.7 | async-start | bytes 1114112 | tf_op jit(solution)/shard_map/all_gather | solution.py:152
  12.0 465.8 %reduce-scatter.2.cloned.1.call-start = ((), (), s32[]{:S(2)}) async-start(), calls=%async_computation.9 | async-start | bytes 1572864 | tf_op jit(solution)/shard_map/reduce_scatter | solution.py:41
  361.4 12.5 %collective-permute-start.2 = (bf16[1,512]{1,0:T(2,128)(2,1)S(1)}, bf16[1,512]{1,0:T(2,128)(2,1)S(1)}, u32[]{:S(2)}, u32[]{:S(2)}) collective-permute-start(bf16[1,512]{1,0:T(2,128)(2,1)S(1)} %get-tuple-element.13), channel_id=1, source_target_pairs={{0,2},{2,4},{4,6},{6,8},{8,10},{10,12},{12,14},{14,16},{16,18},{18... | collective-permute-start | bytes 3080 | tf_op jit(solution)/shard_map/ppermute | solution.py:33
  364.7 9.2 %collective-permute-start.3 = (bf16[1,512]{1,0:T(2,128)(2,1)S(1)}, bf16[1,512]{1,0:T(2,128)(2,1)S(1)}, u32[]{:S(2)}, u32[]{:S(2)}) collective-permute-start(bf16[1,512]{1,0:T(2,128)(2,1)S(1)} %get-tuple-element.14), channel_id=1, source_target_pairs={{2,0},{4,2},{6,4},{8,6},{10,8},{12,10},{14,12},{16,14},{18,16},{20... | collective-permute-start | bytes 3080 | tf_op jit(solution)/shard_map/ppermute | solution.py:34
  366.7 45.9 %collective-permute-start = (bf16[64,512]{1,0:T(8,128)(2,1)}, bf16[64,512]{1,0:T(8,128)(2,1)}, u32[]{:S(2)}, u32[]{:S(2)}) collective-permute-start(bf16[64,512]{1,0:T(8,128)(2,1)} %get-tuple-element.9), channel_id=1, source_target_pairs={{0,2},{2,4},{4,6},{6,8},{8,10},{10,12},{12,14},{14,16},{16,18},{18... | collective-permute-start | bytes 196616 | tf_op jit(solution)/shard_map/ppermute | solution.py:33
  371.8 40.7 %collective-permute-start.1 = (bf16[64,512]{1,0:T(8,128)(2,1)}, bf16[64,512]{1,0:T(8,128)(2,1)}, u32[]{:S(2)}, u32[]{:S(2)}) collective-permute-start(bf16[64,512]{1,0:T(8,128)(2,1)} %get-tuple-element.10), channel_id=1, source_target_pairs={{2,0},{4,2},{6,4},{8,6},{10,8},{12,10},{14,12},{16,14},{18,16},{20... | collective-permute-start | bytes 196616 | tf_op jit(solution)/shard_map/ppermute | solution.py:34
Sparse Core Ops, SparseCore 0:
  10.1 60.4 all-gather.8
  73.3 54.2 all-gather.10
  130.4 53.9 all-gather.12
  187.0 53.9 all-gather.14
  243.5 53.9 all-gather.16
  300.1 53.9 all-gather.18
  356.8 53.9 all-gather.22
  413.6 53.9 all-gather.20
  470.5 7.2 reduce-scatter.1
where the time goes:
time: 487 us; the launch traced here: 486 us
  waiting for transfers between devices  332 us (68%)
  blocking collectives  90.3 us (19%)
  local copies, waits for them, and re-layouts  21.5 us (4%)
  between operations  13.4 us (3%)
  starting transfers between devices  11.4 us (2%)
  matrix products  9.45 us (2%)
  other arithmetic  7.67 us (2%)
    all_gather x1, waiting for transfers between devices, per_device(): lax.all_gather(pre_weight, 'sp', axis=0, tiled=True)  54.4 us
    all_gather x1, waiting for transfers between devices, per_device(): lax.all_gather(post_weight, 'sp', axis=0, tiled=True)  54.3 us
    all_gather x1, waiting for transfers between devices, per_device(): lax.all_gather(attn_gate_weight, 'sp', axis=0, tiled=True)  54.3 us
    all_gather x1, waiting for transfers between devices, per_device(): lax.all_gather(conv_gate_weight, 'sp', axis=0, tiled=True)  54.2 us
    all_gather x1, waiting for transfers between devices, per_device(): lax.all_gather(attn_out_weight, 'sp', axis=1, tiled=True)  50.3 us
    all_gather x1, blocking collectives, per_device(): lax.all_gather(key_weight, 'sp', axis=0, tiled=True)  45.7 us
    all_gather x1, blocking collectives, per_device(): lax.all_gather(value_weight, 'sp', axis=0, tiled=True)  40.2 us
    all_gather x1, waiting for transfers between devices, per_device(): lax.all_gather(conv_out_weight, 'sp', axis=1, tiled=True)  36.9 us
  transfers between devices with their start and end apart: 13, of which 8 were waited for; matrix products, arithmetic and copies ran while one was open for 7% of the time, Pallas kernels for 0%

commit v1 on v0

--- a/solution.py
+++ b/solution.py
@@ -1,6 +1,10 @@
+import functools
+
 import jax
 import jax.numpy as jnp
 from jax import lax
+from jax.experimental import pallas as pl
+from jax.experimental.pallas import tpu as pltpu
 from jax.sharding import PartitionSpec as P
 
 HEAD_DIM = 64
@@ -73,7 +77,7 @@
     )
 
 
-def per_device(
+def gathered_everywhere(
     tokens,
     norm_gain,
     query_weight,
@@ -174,6 +178,378 @@
     ).astype(jnp.bfloat16)
 
 
+MESH = pl.DeviceIdType.MESH
+BF = jnp.bfloat16
+F32 = jnp.float32
+
+
+class Plan:
+    def __init__(self, sp, tp, tokens, query, key, attn_out):
+        self.sp, self.tp = sp, tp
+        self.rows, self.feat = tokens.shape
+        self.members = key.shape[1] // HEAD_DIM
+        self.planes = sp // max(self.members, 1)
+        self.depth = query.shape[0]
+        self.q = query.shape[1] // max(self.members, 1)
+        self.group = query.shape[1] // max(key.shape[1], 1)
+        self.wide = attn_out.shape[1]
+        self.pieces = self.q // max(self.wide, 1)
+        self.all_rows = self.members * self.rows
+
+    def fits(self):
+        m = self.members
+        return (
+            tuple((self.tp, m > 1, self.planes > 1)) == (2, True, True)
+            and self.sp == m * self.planes
+            and self.q == 2 * HEAD_DIM
+            and self.q % 128 == 0
+            and self.feat == m * self.q
+            and self.rows == 2 * WINDOW
+            and self.depth % 16 == 0
+            and self.pieces * self.wide == self.q
+            and self.pieces * m * self.tp == self.sp
+        )
+
+
+def kernel(
+    pl_, tokens_ref, gain_ref, pa_ref, pb_ref, po_ref, sink_ref, taps_ref, o_ref,
+    tok, normed, gain, wa, wb, wo, woa, woc, qb, kvc, postb, act, gates, mix, outb,
+    sends, recvs, local,
+):
+    M, G, T = pl_.members, pl_.planes, pl_.tp
+    R, F, Q, DP = pl_.rows, pl_.feat, pl_.q, pl_.depth
+    H, ALL = WINDOW, pl_.all_rows
+    sp, c = lax.axis_index("sp"), lax.axis_index("tp")
+    g, j = sp // M, lax.rem(sp, M)
+    peer = 1 - c
+
+    others = pl_.sp * T
+    me = sp * T + c
+    barrier = pltpu.get_barrier_semaphore()
+    for d in range(1, others):
+        t = lax.rem(me + d, others)
+        pl.semaphore_signal(barrier, inc=1, device_id=(t // T, lax.rem(t, T)), device_id_type=MESH)
+    pl.semaphore_wait(barrier, others - 1)
+
+    base = {}
+    top = 0
+    for name, count in (
+        ("tok", M), ("lo", 1), ("hi", 1), ("tok2", M), ("lo2", 1), ("hi2", 1), ("gain", 1),
+        ("a", M), ("az", G), ("b", M), ("bz", G), ("wo", pl_.pieces * T),
+        ("act", 2 * M), ("act2", 2 * M), ("out", M),
+    ):
+        base[name] = top
+        top += count
+    waits = []
+
+    def arrived(dst, index):
+        pltpu.make_async_remote_copy(
+            src_ref=dst, dst_ref=dst, send_sem=sends.at[0], recv_sem=recvs.at[index],
+            device_id=(sp, peer), device_id_type=MESH,
+        ).wait_recv()
+
+    def send(src, dst, index, to_sp, to_tp, when=None):
+        copy = pltpu.make_async_remote_copy(
+            src_ref=src, dst_ref=dst, send_sem=sends.at[len(waits)], recv_sem=recvs.at[index],
+            device_id=(to_sp, to_tp), device_id_type=MESH,
+        )
+        waits.append((copy, when))
+        if when is None:
+            copy.start()
+        else:
+            pl.when(when)(lambda: copy.start())
+
+    def al(x, n):
+        return pl.multiple_of(x, n)
+
+    def tok_at(member, half):
+        return tok.at[pl.ds(al(H + member * R, 64), R), pl.ds(al(half * F, 128), F)]
+
+    def lo_at(half):
+        return tok.at[pl.ds(0, H), pl.ds(al(half * F, 128), F)]
+
+    def hi_at(half):
+        return tok.at[pl.ds(H + ALL, H), pl.ds(al(half * F, 128), F)]
+
+    own_copies = []
+
+    def keep(src, dst):
+        copy = pltpu.make_async_copy(src, dst, local.at[len(own_copies)])
+        copy.start()
+        own_copies.append(copy)
+        return copy
+
+    for k in range(1, M):
+        send(tokens_ref, tok_at(j, c), base["tok"] + j, g * M + lax.rem(j + k, M), c)
+    send(tokens_ref, tok_at(j, c), base["tok2"] + j, sp, peer)
+    gain_at = lambda half: gain.at[:, pl.ds(al(half * F, 128), F)]
+    send(gain_ref, gain_at(c), base["gain"], sp, peer)
+    up, down = lax.rem(g + 1, G), lax.rem(g + G - 1, G)
+    for k in range(M):
+        send(tokens_ref.at[pl.ds(R - H, H)], lo_at(c), base["lo"], up * M + k, c, j == M - 1)
+        send(tokens_ref.at[pl.ds(0, H)], hi_at(c), base["hi"], down * M + k, c, j == 0)
+    own_tok = keep(tokens_ref, tok_at(j, c))
+    own_gain = keep(gain_ref, gain_at(c))
+
+    def slot(w, plane, member):
+        return w.at[pl.ds(al((plane * M + member) * DP, 16), DP)]
+
+    def block(w, plane):
+        return w.at[pl.ds(al(plane * M * DP, 16), M * DP)]
+
+    def in_plane(w, packed, name):
+        for k in range(1, M):
+            to = lax.rem(j + k, M)
+            send(packed.at[to], slot(w, g, j), base[name] + j, g * M + to, c)
+        return keep(packed.at[j], slot(w, g, j))
+
+    def own_block(w, name, copy):
+        copy.wait()
+        for k in range(1, M):
+            source = lax.rem(j + M - k, M)
+            arrived(slot(w, g, source), base[name] + source)
+        pass_on(w, name, 0)
+
+    def pass_on(w, name, d):
+        low, high = lax.max(g - d, 0), lax.min(g + d, G - 1)
+        if d > 0:
+            pl.when(g - d >= 0)(lambda: arrived(block(w, low), base[name + "z"] + low))
+        if d < G - 1:
+            send(block(w, low), block(w, low), base[name + "z"] + low,
+                 lax.min(g + 1, G - 1) * M + j, c, (g - d >= 0) & (g < G - 1))
+        if d > 0:
+            pl.when(g + d < G)(lambda: arrived(block(w, high), base[name + "z"] + high))
+        if d < G - 1:
+            send(block(w, high), block(w, high), base[name + "z"] + high,
+                 lax.max(g - 1, 0) * M + j, c, (g + d < G) & (g > 0))
+
+    keep_a = in_plane(wa, pa_ref, "a")
+    keep_b = in_plane(wb, pb_ref, "b")
+    own_block(wa, "a", keep_a)
+
+    for k in range(1, M):
+        source = lax.rem(j + M - k, M)
+        arrived(tok_at(source, c), base["tok"] + source)
+        send(tok_at(source, c), tok_at(source, c), base["tok2"] + source, sp, peer)
+    arrived(lo_at(c), base["lo"])
+    send(lo_at(c), lo_at(c), base["lo2"], sp, peer)
+    arrived(hi_at(c), base["hi"])
+    send(hi_at(c), hi_at(c), base["hi2"], sp, peer)
+    own_tok.wait()
+    own_gain.wait()
+    arrived(gain_at(peer), base["gain"])
+    for k in range(M):
+        arrived(tok_at(k, peer), base["tok2"] + k)
+    arrived(lo_at(peer), base["lo2"])
+    arrived(hi_at(peer), base["hi2"])
+
+    def norm(step, carry):
+        at = pl.ds(al(step * H, 64), H)
+        x = tok[at, :].astype(F32)
+        mean = jnp.sum(x * x, axis=1, keepdims=True) / x.shape[1]
+        normed[at, :] = (x * lax.rsqrt(mean + epsilon) * gain[...]).astype(BF)
+        return carry
+
+    lax.fori_loop(0, (ALL + 2 * H) // H, norm, 0)
+
+    for d in range(1, G - 1):
+        pass_on(wa, "a", d)
+    own_block(wb, "b", keep_b)
+
+    chunk = sp // pl_.pieces
+    piece = lax.rem(sp, pl_.pieces)
+    to_c, to_j = chunk // M, lax.rem(chunk, M)
+    wo_at = lambda i, half: wo.at[i, pl.ds(al(half * F, 128), F)]
+    mine = (to_c == c) & (to_j == j)
+    for k in range(G):
+        to = lax.rem(g + k, G) * M + to_j
+        index = base["wo"] + piece * T + c
+        send(po_ref, wo_at(piece, c), index, to, to_c, None if k else jnp.logical_not(mine))
+    own_wo = pltpu.make_async_copy(po_ref, wo_at(piece, c), recvs.at[base["wo"] + piece * T + c])
+    pl.when(mine)(lambda: own_wo.start())
+
+    pass_on(wa, "a", G - 1)
+
+    def kv_conv(p):
+        kv = p[:, :Q].astype(BF)
+        conv = (p[:, 2 * Q:3 * Q].astype(BF).astype(F32) * p[:, Q:2 * Q].astype(BF).astype(F32))
+        return kv, conv.astype(BF)
+
+    for at, inside in ((0, g > 0), (H + ALL, g < G - 1)):
+        p = jnp.dot(normed[at:at + H, :], wa[:, Q:4 * Q], preferred_element_type=F32)
+        p = jnp.where(inside, p, 0.0)
+        kv, conv = kv_conv(p)
+        kvc[at:at + H, :Q] = kv
+        kvc[at:at + H, Q:] = conv
+
+    def project(m, carry):
+        p = jnp.dot(normed[pl.ds(al(H + m * R, 64), R), :], wa[...], preferred_element_type=F32)
+        kv, conv = kv_conv(p[:, Q:4 * Q])
+        at = pl.ds(al(H + m * R, 64), R)
+        kvc[at, :Q] = kv
+        kvc[at, Q:] = conv
+        here = pl.ds(al(m * R, 128), R)
+        qb[here, :] = p[:, :Q].astype(BF)
+        postb[here, :] = p[:, 4 * Q:].astype(BF)
+        return carry
+
+    lax.fori_loop(0, M, project, 0)
+
+    for d in range(1, G):
+        pass_on(wb, "b", d)
+
+    span = R + 2 * H
+    own = c * M + j
+    act_at = lambda branch, half, member: act.at[
+        :, pl.ds(al(branch * T * F + half * F + member * Q, 128), Q)
+    ]
+    qi = lax.broadcasted_iota(jnp.int32, (R, span), 0)
+    ki = lax.broadcasted_iota(jnp.int32, (R, span), 1)
+    near = jnp.abs(ki - H - qi) <= H
+    taps = taps_ref[:, pl.ds(al(j * Q, 128), Q)]
+
+    def attend(m, carry):
+        here = pl.ds(al(m * R, 128), R)
+        keys = kvc[pl.ds(al(m * R, 64), span), :Q]
+        k_rows, v_rows = keys[:, :HEAD_DIM], keys[:, HEAD_DIM:]
+        kpos = g * ALL + m * R - H + ki
+        allowed = near & (kpos >= 0) & (kpos < G * ALL)
+        queries = qb[here, :]
+        heads = []
+        for h in range(pl_.group):
+            q = queries[:, h * HEAD_DIM:(h + 1) * HEAD_DIM]
+            s = lax.dot_general(q, k_rows, (((1,), (1,)), ((), ())), preferred_element_type=F32)
+            s = jnp.where(allowed, s * HEAD_DIM ** -0.5, negative)
+            sink = sink_ref[0, j * pl_.group + h]
+            high = jnp.maximum(jnp.max(s, axis=1, keepdims=True), sink)
+            e = jnp.exp(s - high)
+            total = jnp.sum(e, axis=1, keepdims=True) + jnp.exp(sink - high)
+            big = e.astype(BF)
+            small = (e - big.astype(F32)).astype(BF)
+            o = jnp.dot(big, v_rows, preferred_element_type=F32)
+            o = o + jnp.dot(small, v_rows, preferred_element_type=F32)
+            heads.append(o / total)
+        act[here, pl.ds(al(own * Q, 128), Q)] = jnp.concatenate(heads, axis=1).astype(BF)
+        x = kvc[pl.ds(al(m * R + H - 16, 16), R + 32), Q:].astype(F32)
+        before = pltpu.roll(x, 1, 0)[16:16 + R]
+        after = pltpu.roll(x, R + 31, 0)[16:16 + R]
+        conv = taps[0:1] * before + taps[1:2] * x[16:16 + R] + taps[2:3] * after
+        conv = postb[here, :].astype(F32) * conv
+        act[here, pl.ds(al(T * F + own * Q, 128), Q)] = conv.astype(BF)
+        return carry
+
+    lax.fori_loop(0, M, attend, 0)
+
+    for b in range(2):
+        for k in range(1, M):
+            send(act_at(b, c, j), act_at(b, c, j), base["act"] + b * M + j, g * M + lax.rem(j + k, M), c)
+        send(act_at(b, c, j), act_at(b, c, j), base["act2"] + b * M + j, sp, peer)
+
+    def gate(m, carry):
+        here = pl.ds(al(m * R, 128), R)
+        p = jnp.dot(normed[pl.ds(al(H + m * R, 64), R), :], wb[...], preferred_element_type=F32)
+        gates[here, :] = jax.nn.sigmoid(p)
+        return carry
+
+    lax.fori_loop(0, M, gate, 0)
+
+    for i in range(pl_.pieces):
+        for half in range(T):
+            arrived(wo_at(i, half), base["wo"] + i * T + half)
+    wide = pl_.wide
+    woa[...] = jnp.concatenate([wo[i, :, :wide] for i in range(pl_.pieces)], axis=1)
+    woc[...] = jnp.concatenate([wo[i, :, wide:] for i in range(pl_.pieces)], axis=1)
+
+    for b in range(2):
+        for k in range(1, M):
+            source = lax.rem(j + M - k, M)
+            arrived(act_at(b, c, source), base["act"] + b * M + source)
+            send(act_at(b, c, source), act_at(b, c, source), base["act2"] + b * M + source, sp, peer)
+    for b in range(2):
+        for k in range(M):
+            arrived(act_at(b, peer, k), base["act2"] + b * M + k)
+
+    for k in range(1, M + 1):
+        m = lax.rem(j + k, M)
+        here = pl.ds(al(m * R, 128), R)
+        attn = jnp.dot(act[here, :T * F], woa[...], preferred_element_type=F32)
+        conv = jnp.dot(act[here, T * F:], woc[...], preferred_element_type=F32)
+        gg = gates[here, :]
+        merged = (gg[:, :Q] * attn + gg[:, Q:] * conv).astype(BF)
+        if k < M:
+            mix[k] = merged
+            send(mix.at[k], outb.at[j], base["out"] + j, g * M + m, c)
+        else:
+            o_ref[:, pl.ds(al(j * Q, 128), Q)] = merged
+    for k in range(1, M):
+        source = lax.rem(j + M - k, M)
+        arrived(outb.at[source], base["out"] + source)
+        o_ref[:, pl.ds(al(source * Q, 128), Q)] = outb[source]
+
+    for copy, when in waits:
+        if when is None:
+            copy.wait_send()
+        else:
+            pl.when(when)(functools.partial(lambda item: item.wait_send(), copy))
+
+
+def in_planes(
+    plan, tokens, norm_gain, query_weight, key_weight, value_weight, conv_in_weight,
+    pre_weight, post_weight, attn_gate_weight, conv_gate_weight, sink_logit, conv_taps,
+    attn_out_weight, conv_out_weight,
+):
+    M, G, T = plan.members, plan.planes, plan.tp
+    R, F, Q, ALL = plan.rows, plan.feat, plan.q, plan.all_rows
+    D = plan.sp * plan.depth
+
+    def packed(*weights):
+        cut = [w.reshape(w.shape[0], M, -1).transpose(1, 0, 2) for w in weights]
+        return jnp.concatenate(cut, axis=2)
+
+    pa = packed(query_weight, key_weight, value_weight, conv_in_weight, pre_weight, post_weight)
+    pb = packed(attn_gate_weight, conv_gate_weight)
+    po = jnp.concatenate([attn_out_weight, conv_out_weight], axis=1)
+    vmem = pl.BlockSpec(memory_space=pltpu.VMEM)
+    span = ALL + 2 * WINDOW
+    return pl.pallas_call(
+        functools.partial(kernel, plan),
+        out_shape=jax.ShapeDtypeStruct(tokens.shape, BF),
+        in_specs=[vmem] * 5 + [pl.BlockSpec(memory_space=pltpu.SMEM), vmem],
+        out_specs=vmem,
+        scratch_shapes=[
+            pltpu.VMEM((span, T * F), BF),
+            pltpu.VMEM((span, T * F), BF),
+            pltpu.VMEM((1, T * F), F32),
+            pltpu.VMEM((D, pa.shape[2]), BF),
+            pltpu.VMEM((D, pb.shape[2]), BF),
+            pltpu.VMEM((plan.pieces, T * F, po.shape[1]), BF),
+            pltpu.VMEM((T * F, Q), BF),
+            pltpu.VMEM((T * F, Q), BF),
+            pltpu.VMEM((ALL, Q), BF),
+            pltpu.VMEM((span, 2 * Q), BF),
+            pltpu.VMEM((ALL, Q), BF),
+            pltpu.VMEM((ALL, 2 * T * F), BF),
+            pltpu.VMEM((ALL, 2 * Q), F32),
+            pltpu.VMEM((M, R, Q), BF),
+            pltpu.VMEM((M, R, Q), BF),
+            pltpu.SemaphoreType.DMA((16 * M + 4 * G + 16,)),
+            pltpu.SemaphoreType.DMA((16 * M + 4 * G + 16,)),
+            pltpu.SemaphoreType.DMA((4,)),
+        ],
+        compiler_params=pltpu.CompilerParams(
+            collective_id=0, has_side_effects=True, vmem_limit_bytes=48 * 1024 * 1024
+        ),
+        name="mixer",
+    )(tokens, norm_gain[None, :], pa, pb, po, sink_logit[None, :], conv_taps)
+
+
+def per_device(*args):
+    plan = Plan(lax.axis_size("sp"), lax.axis_size("tp"), args[0], args[2], args[3], args[12])
+    if plan.fits():
+        return in_planes(plan, *args)
+    return gathered_everywhere(*args)
+
+
 def solution(mesh):
     return jax.shard_map(
         per_device,

time: 487 us -> 90.2 us (0.19)
  waiting for transfers between devices: 332 us -> 0 us
  blocking collectives: 90.3 us -> 0 us
  Pallas kernels: 0 us -> 82.8 us
  local copies, waits for them, and re-layouts: 21.5 us -> 6.77 us
  between operations: 13.4 us -> 0.15 us
  starting transfers between devices: 11.4 us -> 0 us
  matrix products: 9.45 us -> 0 us
  other arithmetic: 7.67 us -> 0.13 us
    all_gather x8 -> x0, waiting for transfers between devices: 320 us -> none  [the longest x1 54.4 us: per_device(): lax.all_gather(pre_weight, 'sp', axis=0, tiled=True)]
    all_gather x3 -> x0, blocking collectives: 87.9 us -> none  [the longest x1 45.7 us: per_device(): lax.all_gather(key_weight, 'sp', axis=0, tiled=True)]
    pallas_call x0 -> x1, Pallas kernels: none -> 82.8 us  [in_planes(): pl.pallas_call(functools.partial(kernel, plan), out_shape=jax.ShapeDtypeS...]
    ppermute x4 -> x0, starting transfers between devices: 11.1 us -> none  [the longest x2 8.5 us: extended(): before = lax.ppermute(last, axis, up)]
    dot_general x5 -> x0, matrix products: 9.45 us -> none  [the longest x1 4.22 us: add_rows(): jnp.dot(segment, rows_here, preferred_element_type=jnp.float32)]
    unnamed x7 -> x29, local copies, waits for them, and re-layouts: 13.4 us -> 5.56 us
    reduce_scatter x1 -> x0, waiting for transfers between devices: 7.4 us -> none  [summed_rows(): return lax.psum_scatter(whole, axis, scatter_dimension=0, tiled=True)]
    unnamed x9 -> x0, waiting for transfers between devices: 5.07 us -> none
  transfers between devices with their start and end apart: 13 -> 0, of which waited for: 8 -> 0; matrix products, arithmetic and copies ran while one was open for 7% -> 0% of each run, Pallas kernels for 0% -> 0%
where the time goes in v1:
time: 90.2 us; the launch traced here: 89.8 us
  Pallas kernels  82.8 us (92%)
  local copies, waits for them, and re-layouts  6.77 us (8%)
    pallas_call x1, Pallas kernels, in_planes(): pl.pallas_call(functools.partial(kernel, plan), out_shape=jax.ShapeDtypeS...  82.8 us
    unnamed x29, local copies, waits for them, and re-layouts  5.56 us

profile of v1, /device:TPU:0, one launch (start us, length us, event | category | flops | bytes accessed | tf_op | source)
XLA Modules:
  0.0 89.8 jit_solution(9119038742453708935)
XLA Ops:
  0.0 0.0 copy-start
  0.0 0.0 copy-start.12
  0.0 0.9 reshape.25
  0.9 0.0 copy-done.12
  0.9 0.1 reshape.26
  1.0 0.0 copy-start.5
  1.1 0.8 copy-done.5
  1.9 0.0 copy-start.6
  1.9 0.1 copy.25
  2.0 0.7 copy-done.6
  2.7 0.1 copy.26
  2.8 0.0 copy-start.7
  2.8 0.1 pad_maximum_fusion.1.po_ref
  3.0 0.0 copy-done
  3.0 0.7 copy-done.7
  3.7 0.8 copy-done.8
  4.5 0.0 copy-done.9
  4.6 0.0 copy-start.10
  4.6 0.0 copy-start.11
  4.6 0.1 concatenate.9.pa_ref
  4.7 0.7 copy-done.10
  5.4 0.0 copy-done.11
  5.5 0.0 copy-start.1
  5.5 0.0 copy-start.2
  5.5 0.0 copy-start.3
  5.5 0.0 copy-start.4
  5.5 0.8 copy-done.1
  6.4 0.0 copy-done.2
  6.4 0.0 copy-done.3
  6.4 0.0 copy-done.4
  6.4 82.8 %mixer.1 = bf16[128,512]{1,0:T(8,128)(2,1)S(1)} custom-call(bf16[128,512]{1,0:T(8,128)(2,1)S(1)} %copy-done.1, f32[1,512]{1,0:T(1,128)S(1)} %bitcast.48, bf16[4,64,640]{2,1,0:T(8,128)(2,1)S(1)} %concatenate.9.pa_ref, bf16[4,64,256]{2,1,0:T(8,128)(2,1)S(1)} %pad_maximum_fusion.pb_ref, bf16[512,128]{1,0:T(8,128)(2,1)S(1)} %pad_maximum_fusion.1.po_ref, ...), custom_call_target="tpu_custom_call" | custom-call | tf_op jit(solution)/shard_map/mixer/pallas_call | solution.py:514
  89.2 0.7 copy.42
  (7 shorter events, 0.1 us)
Async XLA Ops:
  0.0 3.0 %copy-start = (bf16[64,512]{1,0:T(8,128)(2,1)S(1)}, bf16[64,512]{1,0:T(8,128)(2,1)}, u32[]{:S(2)}) copy-start(bf16[64,512]{1,0:T(8,128)(2,1)} %param.16) | copy-start | bytes 196612
  0.0 0.9 %copy-start.12 = (bf16[64,256]{1,0:T(8,128)(2,1)S(1)}, bf16[64,256]{1,0:T(8,128)(2,1)}, u32[]{:S(2)}) copy-start(bf16[64,256]{1,0:T(8,128)(2,1)} %param.18) | copy-start | bytes 98308
  1.0 0.8 copy-start.5
  1.9 0.8 copy-start.6
  2.8 0.8 copy-start.7
  3.7 0.8 copy-start.8
  3.7 0.9 copy-start.9
  4.6 0.8 copy-start.10
  4.6 0.9 copy-start.11
  5.5 0.9 %copy-start.1 = (bf16[128,512]{1,0:T(8,128)(2,1)S(1)}, bf16[128,512]{1,0:T(8,128)(2,1)}, u32[]{:S(2)}) copy-start(bf16[128,512]{1,0:T(8,128)(2,1)} %tokens_ref.1) | copy-start | bytes 393220
  5.5 0.9 copy-start.2
  5.5 0.9 copy-start.3
  5.5 0.9 copy-start.4
